TPU v7x, 32 devices: a whole 2x2x4 slice. The times are simulated.
32 devices in a mesh: tp: 8 (over z, x), dp: 4 (over y, core).
Axes of the slice: x: 2, y: 2, z: 4, core: 2. Of those that a mesh axis runs over, the one named last changes fastest.
Arguments:
- tokens: bfloat16 [112, 4096], P('tp', 'dp'), may hold values from -6 to 6
- w_query: bfloat16 [2, 4096, 4096], P(None, 'dp', 'tp'), may hold values from -0.09375 to 0.09375
- w_key: bfloat16 [2, 4096, 4096], P(None, 'dp', 'tp'), may hold values from -0.09375 to 0.09375
- w_value: bfloat16 [2, 4096, 4096], P(None, 'dp', 'tp'), may hold values from -0.09375 to 0.09375
- w_outgate: bfloat16 [2, 4096, 4096], P(None, 'dp', 'tp'), may hold values from -0.09375 to 0.09375
- w_ingate: bfloat16 [2, 4096, 32], P(None, 'dp'), may hold values from -0.09375 to 0.09375
- w_forget: bfloat16 [2, 4096, 32], P(None, 'dp'), may hold values from -0.09375 to 0.09375
- forget_bias: float32 [2, 32], P(None, 'tp'), may hold values from -2 to 3
- head_gain: float32 [2, 32, 128], P(None, 'tp'), may hold values from 0.1 to 1.9
- w_proj: bfloat16 [2, 4096, 4096], P(None, 'tp', 'dp'), may hold values from -0.09375 to 0.09375
- mem_matrix: float32 [2, 112, 32, 128, 128], P(None, 'dp', 'tp'), may hold values from -0.8 to 0.8
- mem_norm: float32 [2, 112, 32, 128], P(None, 'dp', 'tp'), may hold values from -1.2 to 1.2
- mem_max: float32 [2, 112, 32], P(None, 'dp', 'tp'), may hold values from -4 to 4
Outputs:
- result: bfloat16 [112, 4096], P('tp', 'dp')
- new_matrix: float32 [2, 112, 32, 128, 128], P(None, 'dp', 'tp')
- new_norm: float32 [2, 112, 32, 128], P(None, 'dp', 'tp')
- new_max: float32 [2, 112, 32], P(None, 'dp', 'tp')
All inputs are finite; a program needn't handle non-finite values.
Results may differ from a plain program's by a relative error of at most 0.017.
Values may be sent and summed in bfloat16 or wider, within the bound.
A program may use at most 128 MiB of HBM per device.

v0:
```python
import jax
import jax.numpy as jnp
from jax import lax
from jax.sharding import PartitionSpec as P

HEAD = 128
norm_eps = 1e-06
head_eps = 1e-05


def cell_update(queries, key_vecs, values, log_in, log_forget, matrix, normvec, maxval):
    max_next = jnp.maximum(log_forget + maxval, log_in)
    decays = jnp.exp(log_forget + maxval - max_next)
    weight_in = jnp.exp(log_in - max_next)
    matrix_new = (
        decays[..., None, None] * matrix
        + weight_in[..., None, None] * key_vecs[..., :, None] * values[..., None, :]
    )
    norm_new = decays[..., None] * normvec + weight_in[..., None] * key_vecs
    numerator = jnp.einsum("bhd,bhde->bhe", queries, matrix_new, precision=lax.Precision.HIGHEST)
    denominator = jnp.maximum(jnp.abs(jnp.sum(queries * norm_new, axis=-1)), 1.0)
    return (numerator / denominator[..., None], matrix_new, norm_new, max_next)


def head_norm(readout, gain, outgate):
    average = jnp.mean(readout, axis=-1, keepdims=True)
    variance = jnp.mean(jnp.square(readout - average), axis=-1, keepdims=True)
    normed = (readout - average) * lax.rsqrt(variance + head_eps) * gain
    return normed * jax.nn.sigmoid(outgate)


def mix_block(gathered, weights, states):
    w_query, w_key, w_value, w_outgate, w_ingate, w_forget, bias, gain, w_proj = weights
    matrix, normvec, maxval = states
    features = gathered.shape[1] * lax.axis_size("dp")
    squares = jnp.sum(jnp.square(gathered.astype(jnp.float32)), axis=1)
    heads_dev = bias.shape[0]
    head_start = lax.axis_index("tp") * heads_dev
    gate_in = lax.dynamic_slice_in_dim(w_ingate, head_start, heads_dev, 1)
    gate_forget = lax.dynamic_slice_in_dim(w_forget, head_start, heads_dev, 1)
    part_query = jnp.dot(gathered, w_query, preferred_element_type=jnp.float32)
    part_key = jnp.dot(gathered, w_key, preferred_element_type=jnp.float32)
    part_value = jnp.dot(gathered, w_value, preferred_element_type=jnp.float32)
    part_outgate = jnp.dot(gathered, w_outgate, preferred_element_type=jnp.float32)
    part_ingate = jnp.dot(gathered, gate_in, preferred_element_type=jnp.float32)
    part_forget = jnp.dot(gathered, gate_forget, preferred_element_type=jnp.float32)
    rows_dev = gathered.shape[0] // lax.axis_size("dp")
    totals = lax.psum(squares, "dp")
    own_sum = lax.dynamic_slice_in_dim(totals, lax.axis_index("dp") * rows_dev, rows_dev, 0)
    sum_query, sum_key, sum_value, sum_outgate, sum_ingate, sum_forget = (
        lax.psum_scatter(part_query, "dp", scatter_dimension=0, tiled=True),
        lax.psum_scatter(part_key, "dp", scatter_dimension=0, tiled=True),
        lax.psum_scatter(part_value, "dp", scatter_dimension=0, tiled=True),
        lax.psum_scatter(part_outgate, "dp", scatter_dimension=0, tiled=True),
        lax.psum_scatter(part_ingate, "dp", scatter_dimension=0, tiled=True),
        lax.psum_scatter(part_forget, "dp", scatter_dimension=0, tiled=True),
    )
    inv_scale = lax.rsqrt(own_sum / features + norm_eps)[:, None]
    head_shape = (rows_dev, heads_dev, HEAD)
    queries = (sum_query * inv_scale).reshape(head_shape)
    key_vecs = (sum_key * inv_scale * HEAD ** (-0.5)).reshape(head_shape)
    values = (sum_value * inv_scale).reshape(head_shape)
    outgate = (sum_outgate * inv_scale).reshape(head_shape)
    log_in = sum_ingate * inv_scale
    log_forget = jax.nn.log_sigmoid(sum_forget * inv_scale + bias[None, :])
    readout, matrix_new, norm_new, max_next = cell_update(
        queries, key_vecs, values, log_in, log_forget, matrix, normvec, maxval
    )
    hidden = head_norm(readout, gain[None], outgate).reshape(rows_dev, -1).astype(jnp.bfloat16)
    out_partial = jnp.dot(
        lax.all_gather(hidden, "dp", axis=0, tiled=True), w_proj, preferred_element_type=jnp.float32
    )
    return (out_partial, matrix_new, norm_new, max_next)


def on_device(
    tokens,
    w_query,
    w_key,
    w_value,
    w_outgate,
    w_ingate,
    w_forget,
    forget_bias,
    head_gain,
    w_proj,
    mem_matrix,
    mem_norm,
    mem_max,
):
    current = lax.all_gather(tokens, "tp", axis=0, tiled=True)
    matrix_list, norm_list, max_list = ([], [], [])
    block_total = w_query.shape[0]
    result = current
    for block_id in range(block_total):
        weights = (
            w_query[block_id],
            w_key[block_id],
            w_value[block_id],
            w_outgate[block_id],
            w_ingate[block_id],
            w_forget[block_id],
            forget_bias[block_id],
            head_gain[block_id],
            w_proj[block_id],
        )
        out_partial, matrix_out, norm_out, max_out = mix_block(
            current, weights, (mem_matrix[block_id], mem_norm[block_id], mem_max[block_id])
        )
        matrix_list.append(matrix_out)
        norm_list.append(norm_out)
        max_list.append(max_out)
        if block_id + 1 < block_total:
            current = lax.psum(out_partial, "tp").astype(jnp.bfloat16)
        else:
            result = lax.psum_scatter(
                out_partial.astype(jnp.bfloat16), "tp", scatter_dimension=0, tiled=True
            )
    return (result, jnp.stack(matrix_list), jnp.stack(norm_list), jnp.stack(max_list))


def solution(mesh):
    in_specs = (
        P("tp", "dp"),
        P(None, "dp", "tp"),
        P(None, "dp", "tp"),
        P(None, "dp", "tp"),
        P(None, "dp", "tp"),
        P(None, "dp", None),
        P(None, "dp", None),
        P(None, "tp"),
        P(None, "tp", None),
        P(None, "tp", "dp"),
        P(None, "dp", "tp", None, None),
        P(None, "dp", "tp", None),
        P(None, "dp", "tp"),
    )
    out_specs = (
        P("tp", "dp"),
        P(None, "dp", "tp", None, None),
        P(None, "dp", "tp", None),
        P(None, "dp", "tp"),
    )
    return jax.shard_map(
        on_device, mesh=mesh, in_specs=in_specs, out_specs=out_specs, check_vma=False
    )
```

profile of v0, /device:TPU:0, one launch (start us, length us, event | category | flops | bytes accessed | tf_op | source)
XLA Modules:
  0.0 243.8 jit_solution(15858441146114237513)
XLA Ops:
  0.7 32.9 %all-gather = bf16[8,14,1024]{2,1,0:T(8,128)(2,1)S(1)} all-gather(bf16[1,14,1024]{2,1,0:T(8,128)(2,1)} %bitcast.149), channel_id=1, replica_groups=mesh['tp'=8,'dp'=4] {'tp'}, dimensions={0}, use_global_device_ids=true | all-gather | bytes 258048 | tf_op jit(solution)/shard_map/all_gather | solution.py:91
  33.6 1.5 fusion.36
  35.2 1.5 fusion.38
  36.7 1.5 fusion.40
  38.2 2.4 fusion.42
  40.6 14.0 %fusion.93 = (f32[32,512]{1,0:T(8,128)S(1)}, f32[32,512]{1,0:T(8,128)S(1)}, f32[32,512]{1,0:T(8,128)S(1)}, f32[32,512]{1,0:T(8,128)S(1)}) fusion(f32[112,512]{1,0:T(8,128)S(1)} %fusion.36, f32[112,512]{1,0:T(8,128)} %fusion.42, f32[112,512]{1,0:T(8,128)S(1)} %fusion.38, f32[112,512]{1,0:T(8,128)S(1)} %fusion.40), kind=kCustom, calls=%all-reduce-scatter.10 | all-reduce-scatter fusion | flops 262145 | bytes 1180160
  54.6 1.3 collective-permute-start.1
  55.9 3.7 %collective-permute-start.2 = (f32[12,512]{1,0:T(8,128)S(1)}, f32[12,512]{1,0:T(8,128)S(1)}, u32[]{:S(2)}, u32[]{:S(2)}) collective-permute-start(f32[12,512]{1,0:T(8,128)S(1)} %slice.98), channel_id=1, source_target_pairs={{0,1},{1,2},{2,3},{4,5},{5,6},{6,7},{8,9},{9,10},{10,11},{12,13},{... | collective-permute-start | bytes 73736
  59.6 1.9 collective-permute-start
  61.6 1.9 collective-permute-start.3
  63.6 1.3 slice_bitcast_fusion.2
  64.9 0.9 fusion.99
  66.1 1.3 fusion.100
  68.1 5.8 %all-reduce.23 = (f32[112]{0:T(128)S(1)}, f32[112,4]{0,1:T(4,128)S(1)}, f32[112,4]{0,1:T(4,128)S(1)}) all-reduce(f32[112]{0:T(128)S(1)} %multiply_reduce_fusion.1, f32[112,4]{0,1:T(4,128)S(1)} %convolution_bitcast_fusion.1, f32[112,4]{0,1:T(4,128)S(1)} %convolution_bitcast_fusion), channel_id=1, replica_groups=mesh['tp'=8,'dp'=4] {'dp'}, use_global_device_ids=true, to_apply=%region_2.0 | all-reduce | flops 1008 | bytes 8064 | tf_op jit(solution)/shard_map/psum | solution.py:48
  74.1 0.8 maximum_bitcast_fusion.1
  74.9 0.7 slice_bitcast_fusion
  75.6 1.2 dynamic-slice.64
  78.4 0.2 concatenate.1
  79.4 0.2 fusion.69
  79.7 9.2 %fusion.13 = f32[28,4,1,128]{3,2,1,0:T(1,128)S(1)} fusion(f32[28,4,128,1]{2,3,1,0:T(1,128)S(1)} %bitcast.148, f32[2,28,4,128,128]{4,3,2,1,0:T(8,128)} %param.23, f32[28,4,128]{2,1,0:T(4,128)S(1)} %mul.321, f32[28,4,128]{2,1,0:T(4,128)S(1)} %get-tuple-element.37, f32[28,4]{1,0:T(8,128)S(1)} %copy.41), kind=kOutput, calls=%fused_computation.6 | convolution fusion | flops 27525120 | bytes 7569856 | tf_op jit(solution)/shard_map/bhd,bhde->bhe/dot_general | solution.py:20
  88.9 0.2 fusion.97
  89.4 5.4 %all-gather.1 = bf16[4,28,512]{2,1,0:T(8,128)(2,1)S(1)} all-gather(bf16[1,28,512]{2,1,0:T(8,128)(2,1)S(1)} %reshape.136), channel_id=1, replica_groups=mesh['tp'=8,'dp'=4] {'dp'}, dimensions={0}, use_global_device_ids=true | all-gather | bytes 143360 | tf_op jit(solution)/shard_map/all_gather | solution.py:71
  94.9 0.3 fusion.34
  95.2 43.0 %all-reduce.27 = bf16[112,1024]{1,0:T(8,128)(2,1)S(1)} all-reduce(f32[112,1024]{1,0:T(8,128)S(1)} %fusion.34), channel_id=1, replica_groups=mesh['tp'=8,'dp'=4] {'tp'}, use_global_device_ids=true, to_apply=%region_11.12 | all-reduce | flops 114688 | bytes 688128 | tf_op jit(solution)/shard_map/psum | solution.py:114
  138.4 1.5 fusion.28
  139.9 1.5 fusion.30
  141.4 1.5 fusion.32
  143.0 1.5 fusion.26
  144.8 5.7 %all-reduce.22 = (f32[112]{0:T(128)S(1)}, f32[112,4]{0,1:T(4,128)S(1)}, f32[112,4]{0,1:T(4,128)S(1)}) all-reduce(f32[112]{0:T(128)S(1)} %multiply_reduce_fusion, f32[112,4]{0,1:T(4,128)S(1)} %fusion.72, f32[112,4]{0,1:T(4,128)S(1)} %fusion.70), channel_id=1, replica_groups=mesh['tp'=8,'dp'=4] {'dp'}, use_global_device_ids=true, to_apply=%region_14.15 | all-reduce | flops 1008 | bytes 8064 | tf_op jit(solution)/shard_map/psum | solution.py:48
  150.9 14.6 %fusion.92 = (f32[32,512]{1,0:T(8,128)S(1)}, f32[32,512]{1,0:T(8,128)S(1)}, f32[32,512]{1,0:T(8,128)S(1)}, f32[32,512]{1,0:T(8,128)S(1)}) fusion(f32[112,512]{1,0:T(8,128)S(1)} %fusion.26, f32[112,512]{1,0:T(8,128)S(1)} %fusion.32, f32[112,512]{1,0:T(8,128)S(1)} %fusion.28, f32[112,512]{1,0:T(8,128)S(1)} %fusion.30), kind=kCustom, calls=%all-reduce-scatter.9 | all-reduce-scatter fusion | flops 262145 | bytes 1180160
  165.5 1.3 collective-permute-start.5
  166.8 3.8 %collective-permute-start.6 = (f32[12,512]{1,0:T(8,128)S(1)}, f32[12,512]{1,0:T(8,128)S(1)}, u32[]{:S(2)}, u32[]{:S(2)}) collective-permute-start(f32[12,512]{1,0:T(8,128)S(1)} %slice.102), channel_id=1, source_target_pairs={{0,1},{1,2},{2,3},{4,5},{5,6},{6,7},{8,9},{9,10},{10,11},{12,13},{... | collective-permute-start | bytes 73736
  170.6 1.9 collective-permute-start.4
  172.6 2.1 collective-permute-start.7
  174.7 0.6 pad_maximum_fusion.2
  176.1 0.2 concatenate.7
  176.6 0.2 fusion.66
  176.8 14.1 %multiply_add_fusion.1 = (f32[1,28,4,128,128]{4,3,2,1,0:T(8,128)}, f32[1,28,4,128,128]{4,3,2,1,0:T(8,128)}) fusion(f32[2,28,4,128,128]{4,3,2,1,0:T(8,128)} %param.23, f32[28,4,128]{2,1,0:T(4,128)S(1)} %mul.321, f32[28,4,128]{2,1,0:T(4,128)S(1)} %get-tuple-element.37, f32[28,4]{1,0:T(8,128)S(1)} %copy.41, f32[28,4,128]{2,1,0:T(4,128)S(1)} %mul.347, ...), kind=kLoop, calls=%fused_computation.8 | loop fusion | flops 11010048 | bytes 29590400 | tf_op jit(solution)/shard_map/add | solution.py:16
  190.9 6.9 %fusion.10 = f32[28,4,1,128]{3,2,1,0:T(1,128)S(1)} fusion(f32[28,4,128,1]{2,3,1,0:T(1,128)S(1)} %bitcast.147, f32[2,28,4,128,128]{4,3,2,1,0:T(8,128)S(1)} %bitcast.144, f32[28,4,128]{2,1,0:T(4,128)S(1)} %mul.347, f32[28,4,128]{2,1,0:T(4,128)S(1)} %get-tuple-element.33, f32[28,4]{1,0:T(8,128)S(1)} %copy.44), kind=kOutput, calls=%fused_computation.3 | convolution fusion | flops 27525120 | bytes 7585792 | tf_op jit(solution)/shard_map/bhd,bhde->bhe/dot_general | solution.py:20
  197.9 0.2 fusion.96
  198.4 5.4 %all-gather.2 = bf16[4,28,512]{2,1,0:T(8,128)(2,1)S(1)} all-gather(bf16[1,28,512]{2,1,0:T(8,128)(2,1)S(1)} %reshape.138), channel_id=1, replica_groups=mesh['tp'=8,'dp'=4] {'dp'}, dimensions={0}, use_global_device_ids=true | all-gather | bytes 143360 | tf_op jit(solution)/shard_map/all_gather | solution.py:71
  203.9 1.5 convolution_convert_fusion
  205.4 21.2 %fusion.8 = bf16[16,1024]{1,0:T(8,128)(2,1)S(1)} fusion(bf16[112,1024]{1,0:T(8,128)(2,1)S(1)} %convolution_convert_fusion), kind=kCustom, calls=%all-reduce-scatter.8 | all-reduce-scatter fusion | flops 131073 | bytes 262656
  226.6 2.1 collective-permute-start.8
  228.7 0.2 multiply_add_fusion.3
  228.9 13.4 %pad_maximum_fusion = f32[2,28,4,128,128]{4,3,2,1,0:T(8,128)} fusion(f32[1,28,4,128,128]{4,3,2,1,0:T(8,128)} %get-tuple-element.39, f32[1,28,4,128,128]{4,3,2,1,0:T(8,128)} %get-tuple-element.38), kind=kLoop, calls=%fused_computation | loop fusion | flops 3670016 | bytes 29360128 | tf_op jit(solution)/shard_map/stack | solution.py:119
  242.3 0.7 pad_maximum_fusion.1
  243.1 0.6 constant_dynamic-slice_fusion
  (89 shorter events, 4.4 us)
Async XLA Ops:
  0.6 64.3 %copy-start.2 = (bf16[2,1024,32]{1,2,0:T(8,128)(2,1)S(1)}, bf16[2,1024,32]{1,2,0:T(8,128)(2,1)}, u32[]{:S(2)}) copy-start(bf16[2,1024,32]{1,2,0:T(8,128)(2,1)} %param.18) | copy-start | bytes 393220
  0.6 78.8 %copy-start.1 = (f32[2,28,4,128]{3,2,1,0:T(4,128)S(1)}, f32[2,28,4,128]{3,2,1,0:T(4,128)}, u32[]{:S(2)}) copy-start(f32[2,28,4,128]{3,2,1,0:T(4,128)} %param.24) | copy-start | bytes 344068
  38.2 56.7 %copy-start = (bf16[2,512,1024]{2,1,0:T(8,128)(2,1)S(1)}, bf16[2,512,1024]{2,1,0:T(8,128)(2,1)}, u32[]{:S(2)}) copy-start(bf16[2,512,1024]{2,1,0:T(8,128)(2,1)} %param.22) | copy-start | bytes 6291460
  54.6 23.8 %collective-permute-start.1 = (f32[12,512]{1,0:T(8,128)S(1)}, f32[12,512]{1,0:T(8,128)S(1)}, u32[]{:S(2)}, u32[]{:S(2)}) collective-permute-start(f32[12,512]{1,0:T(8,128)S(1)} %slice.97), channel_id=1, source_target_pairs={{0,1},{1,2},{2,3},{4,5},{5,6},{6,7},{8,9},{9,10},{10,11},{12,13},{... | collective-permute-start | bytes 73736
  55.9 22.6 %collective-permute-start.2 = (f32[12,512]{1,0:T(8,128)S(1)}, f32[12,512]{1,0:T(8,128)S(1)}, u32[]{:S(2)}, u32[]{:S(2)}) collective-permute-start(f32[12,512]{1,0:T(8,128)S(1)} %slice.98), channel_id=1, source_target_pairs={{0,1},{1,2},{2,3},{4,5},{5,6},{6,7},{8,9},{9,10},{10,11},{12,13},{... | collective-permute-start | bytes 73736
  59.6 19.2 %collective-permute-start = (f32[12,512]{1,0:T(8,128)S(1)}, f32[12,512]{1,0:T(8,128)S(1)}, u32[]{:S(2)}, u32[]{:S(2)}) collective-permute-start(f32[12,512]{1,0:T(8,128)S(1)} %slice.96), channel_id=1, source_target_pairs={{0,1},{1,2},{2,3},{4,5},{5,6},{6,7},{8,9},{9,10},{10,11},{12,13},{... | collective-permute-start | bytes 73736
  61.6 17.4 %collective-permute-start.3 = (f32[12,512]{1,0:T(8,128)S(1)}, f32[12,512]{1,0:T(8,128)S(1)}, u32[]{:S(2)}, u32[]{:S(2)}) collective-permute-start(f32[12,512]{1,0:T(8,128)S(1)} %slice.99), channel_id=1, source_target_pairs={{0,1},{1,2},{2,3},{4,5},{5,6},{6,7},{8,9},{9,10},{10,11},{12,13},{... | collective-permute-start | bytes 73736
  79.7 71.0 %copy-start.3 = (f32[2,28,4]{1,2,0:T(4,128)S(1)}, f32[2,28,4]{1,2,0:T(4,128)}, u32[]{:S(2)}) copy-start(f32[2,28,4]{1,2,0:T(4,128)} %param.25) | copy-start | bytes 2692
  79.7 71.0 %copy-start.4 = (f32[4]{0:T(128)S(1)}, f32[4]{0:T(128)}, u32[]{:S(2)}) copy-start(f32[4]{0:T(128)} %get-tuple-element.52) | copy-start | bytes 52
  165.5 10.0 %collective-permute-start.5 = (f32[12,512]{1,0:T(8,128)S(1)}, f32[12,512]{1,0:T(8,128)S(1)}, u32[]{:S(2)}, u32[]{:S(2)}) collective-permute-start(f32[12,512]{1,0:T(8,128)S(1)} %slice.101), channel_id=1, source_target_pairs={{0,1},{1,2},{2,3},{4,5},{5,6},{6,7},{8,9},{9,10},{10,11},{12,13},{... | collective-permute-start | bytes 73736
  166.8 8.9 %collective-permute-start.6 = (f32[12,512]{1,0:T(8,128)S(1)}, f32[12,512]{1,0:T(8,128)S(1)}, u32[]{:S(2)}, u32[]{:S(2)}) collective-permute-start(f32[12,512]{1,0:T(8,128)S(1)} %slice.102), channel_id=1, source_target_pairs={{0,1},{1,2},{2,3},{4,5},{5,6},{6,7},{8,9},{9,10},{10,11},{12,13},{... | collective-permute-start | bytes 73736
  170.6 5.2 %collective-permute-start.4 = (f32[12,512]{1,0:T(8,128)S(1)}, f32[12,512]{1,0:T(8,128)S(1)}, u32[]{:S(2)}, u32[]{:S(2)}) collective-permute-start(f32[12,512]{1,0:T(8,128)S(1)} %slice.100), channel_id=1, source_target_pairs={{0,1},{1,2},{2,3},{4,5},{5,6},{6,7},{8,9},{9,10},{10,11},{12,13},{... | collective-permute-start | bytes 73736
  172.6 3.5 %collective-permute-start.7 = (f32[12,512]{1,0:T(8,128)S(1)}, f32[12,512]{1,0:T(8,128)S(1)}, u32[]{:S(2)}, u32[]{:S(2)}) collective-permute-start(f32[12,512]{1,0:T(8,128)S(1)} %slice.103), channel_id=1, source_target_pairs={{0,1},{1,2},{2,3},{4,5},{5,6},{6,7},{8,9},{9,10},{10,11},{12,13},{... | collective-permute-start | bytes 73736
  176.5 14.4 %slice-start = ((s8[14680064]{0:T(1024)(128)(4,1)}), s8[2097152]{0:T(1024)(128)(4,1)S(1)}, s32[]{:S(2)}) async-start(s8[14680064]{0:T(1024)(128)(4,1)} %bitcast.143), calls=%async_computation | async-start | bytes 4194304
  176.8 14.1 %slice-start.1 = ((s8[14680064]{0:T(1024)(128)(4,1)}), s8[4194304]{0:T(1024)(128)(4,1)S(1)}, s32[]{:S(2)}) async-start(s8[14680064]{0:T(1024)(128)(4,1)} %bitcast.143), calls=%async_computation.1 | async-start | bytes 8388608
  176.8 14.1 %slice-start.2 = ((s8[14680064]{0:T(1024)(128)(4,1)}), s8[4194304]{0:T(1024)(128)(4,1)S(1)}, s32[]{:S(2)}) async-start(s8[14680064]{0:T(1024)(128)(4,1)} %bitcast.143), calls=%async_computation.2 | async-start | bytes 8388608
  176.8 14.1 %slice-start.3 = ((s8[14680064]{0:T(1024)(128)(4,1)}), s8[4194304]{0:T(1024)(128)(4,1)S(1)}, s32[]{:S(2)}) async-start(s8[14680064]{0:T(1024)(128)(4,1)} %bitcast.143), calls=%async_computation.3 | async-start | bytes 8388608
  226.6 16.3 %collective-permute-start.8 = (bf16[14,1024]{1,0:T(8,128)(2,1)S(1)}, bf16[14,1024]{1,0:T(8,128)(2,1)S(1)}, u32[]{:S(2)}, u32[]{:S(2)}) collective-permute-start(bf16[14,1024]{1,0:T(8,128)(2,1)S(1)} %slice.104), channel_id=1, source_target_pairs={{0,4},{4,8},{8,12},{12,16},{16,20},{20,24},{24,28},{1,5},{5,9},{9,... | collective-permute-start | bytes 86024
where the time goes:
time: 245 us; the launch traced here: 244 us
  blocking collectives  148 us (60%)
  other arithmetic  31.9 us (13%)
  matrix products  31.7 us (13%)
  starting transfers between devices  20 us (8%)
  local copies, waits for them, and re-layouts  8.64 us (4%)
  between operations  3.34 us (1%)
    unnamed x3, blocking collectives  49.8 us
    psum x1, blocking collectives, on_device(): current = lax.psum(out_partial, 'tp').astype(jnp.bfloat16)  43 us
    all_gather x1, blocking collectives, on_device(): current = lax.all_gather(tokens, 'tp', axis=0, tiled=True)  32.9 us
    unnamed x9, starting transfers between devices  20 us
    dot_general x2, matrix products, cell_update(): jnp.einsum('bhd,bhde->bhe', queries, matrix_new, precision=lax.Precision....  16.1 us
    add x1, other arithmetic, cell_update(): decays[..., None, None] * matrix  14.1 us
    another operation x1, other arithmetic, on_device(): jnp.stack(matrix_list)  13.4 us
    psum x2, blocking collectives, mix_block(): totals = lax.psum(squares, 'dp')  11.6 us
  transfers between devices with their start and end apart: 9, of which 0 were waited for; matrix products, arithmetic and copies ran while one was open for 10% of the time, Pallas kernels for 0%

commit v1 on v0

--- a/solution.py
+++ b/solution.py
@@ -88,7 +88,14 @@
     mem_norm,
     mem_max,
 ):
-    current = lax.all_gather(tokens, "tp", axis=0, tiled=True)
+    peers = lax.axis_size("tp")
+    right = [(i, (i + 1) % peers) for i in range(peers)]
+    parts = [tokens]
+    for far in range(1, peers):
+        parts = [lax.ppermute(parts[0], "tp", right), *parts]
+    out = jnp.concatenate(parts, axis=0)
+    places = (lax.axis_index("tp") + 1) * parts[-1].shape[0]
+    current = jnp.roll(out, places, axis=0)
     matrix_list, norm_list, max_list = ([], [], [])
     block_total = w_query.shape[0]
     result = current

time: 245 us -> 254 us (1.037)
  waiting for transfers between devices: 0.02 us -> 36.3 us
  blocking collectives: 148 us -> 114 us
  local copies, waits for them, and re-layouts: 8.64 us -> 13.2 us
  starting transfers between devices: 20 us -> 23 us
    ppermute x0 -> x7, waiting for transfers between devices: none -> 36.2 us  [on_device(): parts = [lax.ppermute(parts[0], 'tp', right), *parts]]
    all_gather x1 -> x0, blocking collectives: 32.9 us -> none  [on_device(): current = lax.all_gather(tokens, 'tp', axis=0, tiled=True)]
    concatenate x0 -> x1, local copies, waits for them, and re-layouts: none -> 3.13 us  [on_device(): current = jnp.roll(out, places, axis=0)]
    ppermute x0 -> x7, starting transfers between devices: none -> 3.04 us  [on_device(): parts = [lax.ppermute(parts[0], 'tp', right), *parts]]
    unnamed x44 -> x45, local copies, waits for them, and re-layouts: 5.11 us -> 5.03 us
  transfers between devices with their start and end apart: 9 -> 16, of which waited for: 0 -> 7; matrix products, arithmetic and copies ran while one was open for 10% -> 9% of each run, Pallas kernels for 0% -> 0%
where the time goes in v1:
time: 254 us; the launch traced here: 253 us
  blocking collectives  114 us (45%)
  waiting for transfers between devices  36.3 us (14%)
  matrix products  32.4 us (13%)
  other arithmetic  31.3 us (12%)
  starting transfers between devices  23 us (9%)
  local copies, waits for them, and re-layouts  13.2 us (5%)
  between operations  3.34 us (1%)
    unnamed x3, blocking collectives  49.3 us
    psum x1, blocking collectives, on_device(): current = lax.psum(out_partial, 'tp').astype(jnp.bfloat16)  42.1 us
    ppermute x7, waiting for transfers between devices, on_device(): parts = [lax.ppermute(parts[0], 'tp', right), *parts]  36.2 us
    unnamed x9, starting transfers between devices  20 us
    dot_general x2, matrix products, cell_update(): jnp.einsum('bhd,bhde->bhe', queries, matrix_new, precision=lax.Precision....  16.1 us
    add x1, other arithmetic, cell_update(): decays[..., None, None] * matrix  14.1 us
    another operation x1, other arithmetic, on_device(): jnp.stack(matrix_list)  13.4 us
    psum x2, blocking collectives, mix_block(): totals = lax.psum(squares, 'dp')  11.6 us
  transfers between devices with their start and end apart: 16, of which 7 were waited for; matrix products, arithmetic and copies ran while one was open for 9% of the time, Pallas kernels for 0%

profile of v1, /device:TPU:0, one launch (start us, length us, event | category | flops | bytes accessed | tf_op | source)
XLA Modules:
  0.0 253.3 jit_solution(12684498387717795986)
XLA Ops:
  0.7 3.0 %collective-permute-start = (bf16[14,1024]{1,0:T(8,128)(2,1)}, bf16[14,1024]{1,0:T(8,128)(2,1)S(1)}, u32[]{:S(2)}, u32[]{:S(2)}) collective-permute-start(bf16[14,1024]{1,0:T(8,128)(2,1)} %param.13), channel_id=1, source_target_pairs={{0,4},{4,8},{8,12},{12,16},{16,20},{20,24},{24,28},{28,0},{1,5},{5... | collective-permute-start | bytes 86024 | tf_op jit(solution)/shard_map/ppermute | solution.py:95
  3.7 5.1 %collective-permute-done = bf16[14,1024]{1,0:T(8,128)(2,1)S(1)} collective-permute-done((bf16[14,1024]{1,0:T(8,128)(2,1)}, bf16[14,1024]{1,0:T(8,128)(2,1)S(1)}, u32[]{:S(2)}, u32[]{:S(2)}) %collective-permute-start) | collective-permute-done | bytes 28704 | tf_op jit(solution)/shard_map/ppermute | solution.py:95
  8.8 6.6 %collective-permute-done.1 = bf16[14,1024]{1,0:T(8,128)(2,1)S(1)} collective-permute-done((bf16[14,1024]{1,0:T(8,128)(2,1)S(1)}, bf16[14,1024]{1,0:T(8,128)(2,1)S(1)}, u32[]{:S(2)}, u32[]{:S(2)}) %collective-permute-start.1) | collective-permute-done | bytes 28704 | tf_op jit(solution)/shard_map/ppermute | solution.py:95
  15.4 6.6 %collective-permute-done.2 = bf16[14,1024]{1,0:T(8,128)(2,1)S(1)} collective-permute-done((bf16[14,1024]{1,0:T(8,128)(2,1)S(1)}, bf16[14,1024]{1,0:T(8,128)(2,1)S(1)}, u32[]{:S(2)}, u32[]{:S(2)}) %collective-permute-start.2) | collective-permute-done | bytes 28704 | tf_op jit(solution)/shard_map/ppermute | solution.py:95
  22.0 0.9 fusion.110
  22.9 5.7 %collective-permute-done.3 = bf16[14,1024]{1,0:T(8,128)(2,1)S(1)} collective-permute-done((bf16[14,1024]{1,0:T(8,128)(2,1)S(1)}, bf16[14,1024]{1,0:T(8,128)(2,1)S(1)}, u32[]{:S(2)}, u32[]{:S(2)}) %collective-permute-start.3) | collective-permute-done | bytes 28704 | tf_op jit(solution)/shard_map/ppermute | solution.py:95
  28.7 0.9 fusion.111
  29.5 6.1 %collective-permute-done.4 = bf16[14,1024]{1,0:T(8,128)(2,1)S(1)} collective-permute-done((bf16[14,1024]{1,0:T(8,128)(2,1)S(1)}, bf16[14,1024]{1,0:T(8,128)(2,1)S(1)}, u32[]{:S(2)}, u32[]{:S(2)}) %collective-permute-start.4) | collective-permute-done | bytes 28704 | tf_op jit(solution)/shard_map/ppermute | solution.py:95
  35.6 1.3 slice_bitcast_fusion
  36.9 5.3 %collective-permute-done.5 = bf16[14,1024]{1,0:T(8,128)(2,1)S(1)} collective-permute-done((bf16[14,1024]{1,0:T(8,128)(2,1)S(1)}, bf16[14,1024]{1,0:T(8,128)(2,1)S(1)}, u32[]{:S(2)}, u32[]{:S(2)}) %collective-permute-start.5) | collective-permute-done | bytes 28704 | tf_op jit(solution)/shard_map/ppermute | solution.py:95
  42.2 1.3 slice_bitcast_fusion.2
  43.6 1.2 dynamic-slice.64
  45.4 1.3 fusion.112
  48.1 0.8 collective-permute-done.6
  48.8 3.1 %concatenate.6 = bf16[224,1024]{1,0:T(8,128)(2,1)S(1)} concatenate(bf16[14,1024]{1,0:T(8,128)(2,1)S(1)} %collective-permute-done.6, bf16[14,1024]{1,0:T(8,128)(2,1)S(1)} %collective-permute-done.5, bf16[14,1024]{1,0:T(8,128)(2,1)S(1)} %collective-permute-done.4, bf16[14,1024]{1,0:T(8,128)(2,1)S(1)} %collective-permute-done.3, bf16[14,1024]{1,0:T(8,128)(2,1)S(1)} %collective-permute-done.2, ...), dimensions={0} | concatenate | bytes 917504 | tf_op jit(solution)/shard_map/jit(_roll_dynamic)/concatenate | solution.py:98
  52.5 1.5 fusion.40
  54.0 1.5 fusion.38
  55.6 2.4 fusion.36
  58.0 2.2 fusion.42
  60.2 13.9 %fusion.105 = (f32[32,512]{1,0:T(8,128)S(1)}, f32[32,512]{1,0:T(8,128)S(1)}, f32[32,512]{1,0:T(8,128)S(1)}, f32[32,512]{1,0:T(8,128)S(1)}) fusion(f32[112,512]{1,0:T(8,128)} %fusion.36, f32[112,512]{1,0:T(8,128)} %fusion.42, f32[112,512]{1,0:T(8,128)S(1)} %fusion.38, f32[112,512]{1,0:T(8,128)S(1)} %fusion.40), kind=kCustom, calls=%all-reduce-scatter.10 | all-reduce-scatter fusion | flops 262145 | bytes 1180160
  74.2 1.3 collective-permute-start.8
  75.5 3.7 %collective-permute-start.9 = (f32[12,512]{1,0:T(8,128)S(1)}, f32[12,512]{1,0:T(8,128)S(1)}, u32[]{:S(2)}, u32[]{:S(2)}) collective-permute-start(f32[12,512]{1,0:T(8,128)S(1)} %slice.98), channel_id=1, source_target_pairs={{0,1},{1,2},{2,3},{4,5},{5,6},{6,7},{8,9},{9,10},{10,11},{12,13},{... | collective-permute-start | bytes 73736
  79.2 1.9 collective-permute-start.7
  81.1 1.9 collective-permute-start.10
  83.0 5.8 %all-reduce.23 = (f32[112]{0:T(128)S(1)}, f32[112,4]{0,1:T(4,128)S(1)}, f32[112,4]{0,1:T(4,128)S(1)}) all-reduce(f32[112]{0:T(128)S(1)} %multiply_reduce_fusion.1, f32[112,4]{0,1:T(4,128)S(1)} %fusion.69, f32[112,4]{0,1:T(4,128)S(1)} %fusion.67), channel_id=1, replica_groups=mesh['tp'=8,'dp'=4] {'dp'}, use_global_device_ids=true, to_apply=%region_2.3 | all-reduce | flops 1008 | bytes 8064 | tf_op jit(solution)/shard_map/psum | solution.py:48
  90.6 9.2 %fusion.13 = f32[28,4,1,128]{3,2,1,0:T(1,128)S(1)} fusion(f32[28,4,128,1]{2,3,1,0:T(1,128)S(1)} %bitcast.137, f32[2,28,4,128,128]{4,3,2,1,0:T(8,128)} %param.23, f32[28,4,128]{2,1,0:T(4,128)S(1)} %mul.325, f32[28,4,128]{2,1,0:T(4,128)S(1)} %get-tuple-element.37, f32[28,4]{1,0:T(8,128)S(1)} %copy.41), kind=kOutput, calls=%fused_computation.6 | convolution fusion | flops 27525120 | bytes 7569856 | tf_op jit(solution)/shard_map/bhd,bhde->bhe/dot_general | solution.py:20
  100.4 5.4 %all-gather = bf16[4,28,512]{2,1,0:T(8,128)(2,1)S(1)} all-gather(bf16[1,28,512]{2,1,0:T(8,128)(2,1)S(1)} %reshape.134), channel_id=1, replica_groups=mesh['tp'=8,'dp'=4] {'dp'}, dimensions={0}, use_global_device_ids=true | all-gather | bytes 143360 | tf_op jit(solution)/shard_map/all_gather | solution.py:71
  106.1 42.1 %all-reduce.27 = bf16[112,1024]{1,0:T(8,128)(2,1)S(1)} all-reduce(f32[112,1024]{1,0:T(8,128)S(1)} %fusion.34), channel_id=1, replica_groups=mesh['tp'=8,'dp'=4] {'tp'}, use_global_device_ids=true, to_apply=%region_11.12 | all-reduce | flops 114688 | bytes 688128 | tf_op jit(solution)/shard_map/psum | solution.py:121
  148.4 1.5 fusion.28
  149.9 1.5 fusion.30
  151.4 1.5 fusion.32
  153.0 1.5 fusion.26
  154.8 5.7 %all-reduce.22 = (f32[112]{0:T(128)S(1)}, f32[112,4]{0,1:T(4,128)S(1)}, f32[112,4]{0,1:T(4,128)S(1)}) all-reduce(f32[112]{0:T(128)S(1)} %multiply_reduce_fusion, f32[112,4]{0,1:T(4,128)S(1)} %fusion.80, f32[112,4]{0,1:T(4,128)S(1)} %fusion.78), channel_id=1, replica_groups=mesh['tp'=8,'dp'=4] {'dp'}, use_global_device_ids=true, to_apply=%region_14.15 | all-reduce | flops 1008 | bytes 8064 | tf_op jit(solution)/shard_map/psum | solution.py:48
  160.8 14.6 %fusion.104 = (f32[32,512]{1,0:T(8,128)S(1)}, f32[32,512]{1,0:T(8,128)S(1)}, f32[32,512]{1,0:T(8,128)S(1)}, f32[32,512]{1,0:T(8,128)S(1)}) fusion(f32[112,512]{1,0:T(8,128)S(1)} %fusion.26, f32[112,512]{1,0:T(8,128)S(1)} %fusion.32, f32[112,512]{1,0:T(8,128)S(1)} %fusion.28, f32[112,512]{1,0:T(8,128)S(1)} %fusion.30), kind=kCustom, calls=%all-reduce-scatter.9 | all-reduce-scatter fusion | flops 262145 | bytes 1180160
  175.5 1.3 collective-permute-start.12
  176.8 3.8 %collective-permute-start.13 = (f32[12,512]{1,0:T(8,128)S(1)}, f32[12,512]{1,0:T(8,128)S(1)}, u32[]{:S(2)}, u32[]{:S(2)}) collective-permute-start(f32[12,512]{1,0:T(8,128)S(1)} %slice.102), channel_id=1, source_target_pairs={{0,1},{1,2},{2,3},{4,5},{5,6},{6,7},{8,9},{9,10},{10,11},{12,13},{... | collective-permute-start | bytes 73736
  180.6 1.9 collective-permute-start.11
  182.5 2.1 collective-permute-start.14
  184.7 0.6 pad_maximum_fusion.2
  186.8 14.1 %multiply_add_fusion.1 = (f32[1,28,4,128,128]{4,3,2,1,0:T(8,128)}, f32[1,28,4,128,128]{4,3,2,1,0:T(8,128)}) fusion(f32[2,28,4,128,128]{4,3,2,1,0:T(8,128)} %param.23, f32[28,4,128]{2,1,0:T(4,128)S(1)} %mul.325, f32[28,4,128]{2,1,0:T(4,128)S(1)} %get-tuple-element.37, f32[28,4]{1,0:T(8,128)S(1)} %copy.41, f32[28,4,128]{2,1,0:T(4,128)S(1)} %mul.351, ...), kind=kLoop, calls=%fused_computation.8 | loop fusion | flops 11010048 | bytes 29590400 | tf_op jit(solution)/shard_map/add | solution.py:16
  200.9 6.9 %fusion.10 = f32[28,4,1,128]{3,2,1,0:T(1,128)S(1)} fusion(f32[28,4,128,1]{2,3,1,0:T(1,128)S(1)} %bitcast.136, f32[2,28,4,128,128]{4,3,2,1,0:T(8,128)S(1)} %bitcast.133, f32[28,4,128]{2,1,0:T(4,128)S(1)} %mul.351, f32[28,4,128]{2,1,0:T(4,128)S(1)} %get-tuple-element.33, f32[28,4]{1,0:T(8,128)S(1)} %copy.44), kind=kOutput, calls=%fused_computation.3 | convolution fusion | flops 27525120 | bytes 7585792 | tf_op jit(solution)/shard_map/bhd,bhde->bhe/dot_general | solution.py:20
  208.4 5.4 %all-gather.1 = bf16[4,28,512]{2,1,0:T(8,128)(2,1)S(1)} all-gather(bf16[1,28,512]{2,1,0:T(8,128)(2,1)S(1)} %reshape.136), channel_id=1, replica_groups=mesh['tp'=8,'dp'=4] {'dp'}, dimensions={0}, use_global_device_ids=true | all-gather | bytes 143360 | tf_op jit(solution)/shard_map/all_gather | solution.py:71
  213.9 1.5 convolution_convert_fusion
  215.4 20.8 %fusion.8 = bf16[16,1024]{1,0:T(8,128)(2,1)S(1)} fusion(bf16[112,1024]{1,0:T(8,128)(2,1)S(1)} %convolution_convert_fusion), kind=kCustom, calls=%all-reduce-scatter.8 | all-reduce-scatter fusion | flops 131073 | bytes 262656
  236.2 2.0 collective-permute-start.15
  238.4 13.4 %pad_maximum_fusion = f32[2,28,4,128,128]{4,3,2,1,0:T(8,128)} fusion(f32[1,28,4,128,128]{4,3,2,1,0:T(8,128)} %get-tuple-element.39, f32[1,28,4,128,128]{4,3,2,1,0:T(8,128)} %get-tuple-element.38), kind=kLoop, calls=%fused_computation | loop fusion | flops 3670016 | bytes 29360128 | tf_op jit(solution)/shard_map/stack | solution.py:126
  251.8 0.7 pad_maximum_fusion.1
  252.7 0.6 constant_dynamic-slice_fusion
  (104 shorter events, 6.2 us)
Async XLA Ops:
  0.6 88.3 %copy-start.3 = (f32[2,28,4]{1,2,0:T(4,128)S(1)}, f32[2,28,4]{1,2,0:T(4,128)}, u32[]{:S(2)}) copy-start(f32[2,28,4]{1,2,0:T(4,128)} %param.25) | copy-start | bytes 2692
  0.6 89.7 %copy-start.1 = (f32[2,28,4,128]{3,2,1,0:T(4,128)S(1)}, f32[2,28,4,128]{3,2,1,0:T(4,128)}, u32[]{:S(2)}) copy-start(f32[2,28,4,128]{3,2,1,0:T(4,128)} %param.24) | copy-start | bytes 344068
  0.7 8.2 %collective-permute-start = (bf16[14,1024]{1,0:T(8,128)(2,1)}, bf16[14,1024]{1,0:T(8,128)(2,1)S(1)}, u32[]{:S(2)}, u32[]{:S(2)}) collective-permute-start(bf16[14,1024]{1,0:T(8,128)(2,1)} %param.13), channel_id=1, source_target_pairs={{0,4},{4,8},{8,12},{12,16},{16,20},{20,24},{24,28},{28,0},{1,5},{5... | collective-permute-start | bytes 86024 | tf_op jit(solution)/shard_map/ppermute | solution.py:95
  8.8 6.6 %collective-permute-start.1 = (bf16[14,1024]{1,0:T(8,128)(2,1)S(1)}, bf16[14,1024]{1,0:T(8,128)(2,1)S(1)}, u32[]{:S(2)}, u32[]{:S(2)}) collective-permute-start(bf16[14,1024]{1,0:T(8,128)(2,1)S(1)} %collective-permute-done), channel_id=1, source_target_pairs={{0,4},{4,8},{8,12},{12,16},{16,20},{20,24},{24,28},{28,0},{1,5},{5... | collective-permute-start | bytes 86024 | tf_op jit(solution)/shard_map/ppermute | solution.py:95
  15.4 6.6 %collective-permute-start.2 = (bf16[14,1024]{1,0:T(8,128)(2,1)S(1)}, bf16[14,1024]{1,0:T(8,128)(2,1)S(1)}, u32[]{:S(2)}, u32[]{:S(2)}) collective-permute-start(bf16[14,1024]{1,0:T(8,128)(2,1)S(1)} %collective-permute-done.1), channel_id=1, source_target_pairs={{0,4},{4,8},{8,12},{12,16},{16,20},{20,24},{24,28},{28,0},{1,5},{5... | collective-permute-start | bytes 86024 | tf_op jit(solution)/shard_map/ppermute | solution.py:95
  22.0 6.6 %collective-permute-start.3 = (bf16[14,1024]{1,0:T(8,128)(2,1)S(1)}, bf16[14,1024]{1,0:T(8,128)(2,1)S(1)}, u32[]{:S(2)}, u32[]{:S(2)}) collective-permute-start(bf16[14,1024]{1,0:T(8,128)(2,1)S(1)} %collective-permute-done.2), channel_id=1, source_target_pairs={{0,4},{4,8},{8,12},{12,16},{16,20},{20,24},{24,28},{28,0},{1,5},{5... | collective-permute-start | bytes 86024 | tf_op jit(solution)/shard_map/ppermute | solution.py:95
  28.7 7.0 %collective-permute-start.4 = (bf16[14,1024]{1,0:T(8,128)(2,1)S(1)}, bf16[14,1024]{1,0:T(8,128)(2,1)S(1)}, u32[]{:S(2)}, u32[]{:S(2)}) collective-permute-start(bf16[14,1024]{1,0:T(8,128)(2,1)S(1)} %collective-permute-done.3), channel_id=1, source_target_pairs={{0,4},{4,8},{8,12},{12,16},{16,20},{20,24},{24,28},{28,0},{1,5},{5... | collective-permute-start | bytes 86024 | tf_op jit(solution)/shard_map/ppermute | solution.py:95
  35.6 6.6 %collective-permute-start.5 = (bf16[14,1024]{1,0:T(8,128)(2,1)S(1)}, bf16[14,1024]{1,0:T(8,128)(2,1)S(1)}, u32[]{:S(2)}, u32[]{:S(2)}) collective-permute-start(bf16[14,1024]{1,0:T(8,128)(2,1)S(1)} %collective-permute-done.4), channel_id=1, source_target_pairs={{0,4},{4,8},{8,12},{12,16},{16,20},{20,24},{24,28},{28,0},{1,5},{5... | collective-permute-start | bytes 86024 | tf_op jit(solution)/shard_map/ppermute | solution.py:95
  42.2 6.6 %collective-permute-start.6 = (bf16[14,1024]{1,0:T(8,128)(2,1)S(1)}, bf16[14,1024]{1,0:T(8,128)(2,1)S(1)}, u32[]{:S(2)}, u32[]{:S(2)}) collective-permute-start(bf16[14,1024]{1,0:T(8,128)(2,1)S(1)} %collective-permute-done.5), channel_id=1, source_target_pairs={{0,4},{4,8},{8,12},{12,16},{16,20},{20,24},{24,28},{28,0},{1,5},{5... | collective-permute-start | bytes 86024 | tf_op jit(solution)/shard_map/ppermute | solution.py:95
  55.6 50.2 %copy-start = (bf16[2,512,1024]{2,1,0:T(8,128)(2,1)S(1)}, bf16[2,512,1024]{2,1,0:T(8,128)(2,1)}, u32[]{:S(2)}) copy-start(bf16[2,512,1024]{2,1,0:T(8,128)(2,1)} %param.22) | copy-start | bytes 6291460
  74.2 15.2 %collective-permute-start.8 = (f32[12,512]{1,0:T(8,128)S(1)}, f32[12,512]{1,0:T(8,128)S(1)}, u32[]{:S(2)}, u32[]{:S(2)}) collective-permute-start(f32[12,512]{1,0:T(8,128)S(1)} %slice.97), channel_id=1, source_target_pairs={{0,1},{1,2},{2,3},{4,5},{5,6},{6,7},{8,9},{9,10},{10,11},{12,13},{... | collective-permute-start | bytes 73736
  75.5 14.1 %collective-permute-start.9 = (f32[12,512]{1,0:T(8,128)S(1)}, f32[12,512]{1,0:T(8,128)S(1)}, u32[]{:S(2)}, u32[]{:S(2)}) collective-permute-start(f32[12,512]{1,0:T(8,128)S(1)} %slice.98), channel_id=1, source_target_pairs={{0,1},{1,2},{2,3},{4,5},{5,6},{6,7},{8,9},{9,10},{10,11},{12,13},{... | collective-permute-start | bytes 73736
  79.2 10.6 %collective-permute-start.7 = (f32[12,512]{1,0:T(8,128)S(1)}, f32[12,512]{1,0:T(8,128)S(1)}, u32[]{:S(2)}, u32[]{:S(2)}) collective-permute-start(f32[12,512]{1,0:T(8,128)S(1)} %slice.96), channel_id=1, source_target_pairs={{0,1},{1,2},{2,3},{4,5},{5,6},{6,7},{8,9},{9,10},{10,11},{12,13},{... | collective-permute-start | bytes 73736
  81.1 8.8 %collective-permute-start.10 = (f32[12,512]{1,0:T(8,128)S(1)}, f32[12,512]{1,0:T(8,128)S(1)}, u32[]{:S(2)}, u32[]{:S(2)}) collective-permute-start(f32[12,512]{1,0:T(8,128)S(1)} %slice.99), channel_id=1, source_target_pairs={{0,1},{1,2},{2,3},{4,5},{5,6},{6,7},{8,9},{9,10},{10,11},{12,13},{... | collective-permute-start | bytes 73736
  90.6 70.1 %copy-start.4 = (f32[2,28,4]{1,2,0:T(4,128)S(1)}, f32[2,28,4]{1,2,0:T(4,128)}, u32[]{:S(2)}) copy-start(f32[2,28,4]{1,2,0:T(4,128)} %param.25) | copy-start | bytes 2692
  90.6 70.1 %copy-start.5 = (f32[4]{0:T(128)S(1)}, f32[4]{0:T(128)}, u32[]{:S(2)}) copy-start(f32[4]{0:T(128)} %get-tuple-element.52) | copy-start | bytes 52
  175.5 10.0 %collective-permute-start.12 = (f32[12,512]{1,0:T(8,128)S(1)}, f32[12,512]{1,0:T(8,128)S(1)}, u32[]{:S(2)}, u32[]{:S(2)}) collective-permute-start(f32[12,512]{1,0:T(8,128)S(1)} %slice.101), channel_id=1, source_target_pairs={{0,1},{1,2},{2,3},{4,5},{5,6},{6,7},{8,9},{9,10},{10,11},{12,13},{... | collective-permute-start | bytes 73736
  176.8 8.9 %collective-permute-start.13 = (f32[12,512]{1,0:T(8,128)S(1)}, f32[12,512]{1,0:T(8,128)S(1)}, u32[]{:S(2)}, u32[]{:S(2)}) collective-permute-start(f32[12,512]{1,0:T(8,128)S(1)} %slice.102), channel_id=1, source_target_pairs={{0,1},{1,2},{2,3},{4,5},{5,6},{6,7},{8,9},{9,10},{10,11},{12,13},{... | collective-permute-start | bytes 73736
  180.6 5.2 %collective-permute-start.11 = (f32[12,512]{1,0:T(8,128)S(1)}, f32[12,512]{1,0:T(8,128)S(1)}, u32[]{:S(2)}, u32[]{:S(2)}) collective-permute-start(f32[12,512]{1,0:T(8,128)S(1)} %slice.100), channel_id=1, source_target_pairs={{0,1},{1,2},{2,3},{4,5},{5,6},{6,7},{8,9},{9,10},{10,11},{12,13},{... | collective-permute-start | bytes 73736
  182.5 3.5 %collective-permute-start.14 = (f32[12,512]{1,0:T(8,128)S(1)}, f32[12,512]{1,0:T(8,128)S(1)}, u32[]{:S(2)}, u32[]{:S(2)}) collective-permute-start(f32[12,512]{1,0:T(8,128)S(1)} %slice.103), channel_id=1, source_target_pairs={{0,1},{1,2},{2,3},{4,5},{5,6},{6,7},{8,9},{9,10},{10,11},{12,13},{... | collective-permute-start | bytes 73736
  186.5 14.4 %slice-start = ((s8[14680064]{0:T(1024)(128)(4,1)}), s8[2097152]{0:T(1024)(128)(4,1)S(1)}, s32[]{:S(2)}) async-start(s8[14680064]{0:T(1024)(128)(4,1)} %bitcast.132), calls=%async_computation | async-start | bytes 4194304
  186.8 14.1 %slice-start.1 = ((s8[14680064]{0:T(1024)(128)(4,1)}), s8[4194304]{0:T(1024)(128)(4,1)S(1)}, s32[]{:S(2)}) async-start(s8[14680064]{0:T(1024)(128)(4,1)} %bitcast.132), calls=%async_computation.1 | async-start | bytes 8388608
  186.8 14.1 %slice-start.2 = ((s8[14680064]{0:T(1024)(128)(4,1)}), s8[4194304]{0:T(1024)(128)(4,1)S(1)}, s32[]{:S(2)}) async-start(s8[14680064]{0:T(1024)(128)(4,1)} %bitcast.132), calls=%async_computation.2 | async-start | bytes 8388608
  186.8 14.1 %slice-start.3 = ((s8[14680064]{0:T(1024)(128)(4,1)}), s8[4194304]{0:T(1024)(128)(4,1)S(1)}, s32[]{:S(2)}) async-start(s8[14680064]{0:T(1024)(128)(4,1)} %bitcast.132), calls=%async_computation.3 | async-start | bytes 8388608
  200.9 7.4 %copy-start.2 = (f32[4,128]{1,0:T(4,128)S(1)}, f32[4,128]{1,0:T(4,128)}, u32[]{:S(2)}) copy-start(f32[4,128]{1,0:T(4,128)} %get-tuple-element.50) | copy-start | bytes 6148
  236.2 16.2 %collective-permute-start.15 = (bf16[14,1024]{1,0:T(8,128)(2,1)S(1)}, bf16[14,1024]{1,0:T(8,128)(2,1)S(1)}, u32[]{:S(2)}, u32[]{:S(2)}) collective-permute-start(bf16[14,1024]{1,0:T(8,128)(2,1)S(1)} %slice.104), channel_id=1, source_target_pairs={{0,4},{4,8},{8,12},{12,16},{16,20},{20,24},{24,28},{1,5},{5,9},{9,... | collective-permute-start | bytes 86024
